TPU v7x, 32 devices: a whole 2x2x4 slice. The times are simulated.
32 devices in a mesh: sp: 8 (over z, y), tp: 4 (over x, core).
Axes of the slice: x: 2, y: 2, z: 4, core: 2. Of those that a mesh axis runs over, the one named last changes fastest.
Arguments:
- tokens_in: bfloat16 [2048, 2048], P('sp'), may hold values from -3 to 3
- queries: bfloat16 [2048, 1024], P('sp', 'tp'), may hold values from -6 to 6
- keys: bfloat16 [2048, 256], P('sp', 'tp'), may hold values from -6 to 6
- values: bfloat16 [2048, 256], P('sp', 'tp'), may hold values from -12 to 12
- doc_ids: int32 [2048], P('sp'), may hold values from 0 to 1, never falling along the last dimension, each value on 1 to 1280 neighbouring positions
- query_gain: float32 [64], replicated, may hold values from 2.5 to 6
- key_norm_scale: float32 [64], replicated, may hold values from 2.5 to 6
- out_weight: bfloat16 [1024, 2048], P('tp'), may hold values from -0.1875 to 0.1875
- norm_gain: float32 [2048], replicated, may hold values from 0.1 to 1.9
- gate_weight: bfloat16 [2048, 5632], P('sp', 'tp'), may hold values from -0.125 to 0.125
- up_weight: bfloat16 [2048, 5632], P('sp', 'tp'), may hold values from -0.125 to 0.125
- down_weight: bfloat16 [5632, 2048], P('tp', 'sp'), may hold values from -0.078125 to 0.078125
Outputs:
- layer_out: bfloat16 [2048, 2048], P('sp')
Inputs may be any that keep to these rules, and one draw needn't show every extreme that they name: `doc_ids`: document numbers never fall along the sequence; every document has 1 to 1280 positions and one has exactly 1280.
All inputs are finite; a program needn't handle non-finite values.
Results may differ from a plain program's by a relative error of at most 0.014.
The roundings to bfloat16 on the way count: a program that leaves them out, or rounds other values in their place, can miss the bound.
Values may be sent and summed in bfloat16 or wider, within the bound.
A program may use at most 128 MiB of HBM per device.

v0:
```python
import jax
import jax.numpy as jnp
from jax import lax
from jax.sharding import PartitionSpec as P

GRID = 64


EPS = 1e-06
THETA = 10000.0
NEG = -1e30


def rotate_half(block, angle):
    half_dim = block.shape[-1] // 2
    cosine = jnp.cos(angle)[:, None, :]
    sine = jnp.sin(angle)[:, None, :]
    first = block[..., :half_dim]
    second = block[..., half_dim:]
    return jnp.concatenate(
        [first * cosine - second * sine, second * cosine + first * sine], axis=-1
    )


def normalized_rotated(values_in, gain, heads, lattice_row, lattice_column):
    full = values_in.astype(jnp.float32).reshape(values_in.shape[0], heads, -1)
    full = full * lax.rsqrt(jnp.mean(full * full, axis=-1, keepdims=True) + EPS) * gain
    half_dim = full.shape[-1] // 2
    freqs = THETA ** (-2.0 * jnp.arange(half_dim // 2, dtype=jnp.float32) / half_dim)
    by_row = rotate_half(full[..., :half_dim], lattice_row[:, None] * freqs[None, :])
    by_col = rotate_half(full[..., half_dim:], lattice_column[:, None] * freqs[None, :])
    return jnp.concatenate([by_row, by_col], axis=-1).astype(jnp.bfloat16)


def per_device(
    tokens_in,
    queries,
    keys,
    values,
    doc_ids,
    query_gain,
    key_norm_scale,
    out_weight,
    norm_gain,
    gate_weight,
    up_weight,
    down_weight,
):
    tok_rows = tokens_in.shape[0]
    head_dim = query_gain.shape[0]
    local_heads = queries.shape[1] // head_dim
    places = lax.axis_index("sp") * tok_rows + jnp.arange(tok_rows, dtype=jnp.int32)
    lattice_row = (places // GRID).astype(jnp.float32)
    lattice_column = (places % GRID).astype(jnp.float32)
    q_local = normalized_rotated(queries, query_gain, local_heads, lattice_row, lattice_column)
    q_rows = q_local.transpose(1, 0, 2).reshape(local_heads * tok_rows, head_dim)
    key_pairs = normalized_rotated(keys, key_norm_scale, 1, lattice_row, lattice_column).reshape(
        tok_rows // 2, 2 * head_dim
    )
    value_pairs = values.reshape(tok_rows // 2, 2 * head_dim)
    doc_pairs = doc_ids.reshape(tok_rows // 2, 2)
    row_docs = jnp.tile(doc_ids, local_heads)
    first_doc = doc_ids[0]
    last_doc = doc_ids[-1]
    scale = head_dim ** (-0.5)
    total_rows = local_heads * tok_rows

    def absorb_block(state, key_block, value_block, doc_block):

        def absorb(current):
            running_max, running_sum, running_acc = current
            scores = (
                jnp.einsum("qd,kd->qk", q_rows, key_block, preferred_element_type=jnp.float32)
                * scale
            )
            same = row_docs[:, None] == doc_block[None, :]
            scores = jnp.where(same, scores, NEG)
            new_max = jnp.maximum(running_max, jnp.max(scores, axis=1))
            weights = jnp.where(same, jnp.exp(scores - new_max[:, None]), 0.0)
            shrink = jnp.exp(running_max - new_max)
            new_sum = running_sum * shrink + jnp.sum(weights, axis=1)
            new_acc = running_acc * shrink[:, None] + jnp.dot(
                weights.astype(jnp.bfloat16), value_block, preferred_element_type=jnp.float32
            )
            return (new_max, new_sum, new_acc)

        touches = (doc_block[0] <= last_doc) & (doc_block[-1] >= first_doc)
        return lax.cond(touches, absorb, lambda current: current, state)

    initial = (
        jnp.full((total_rows,), NEG, jnp.float32),
        jnp.zeros((total_rows,), jnp.float32),
        jnp.zeros((total_rows, head_dim), jnp.float32),
    )
    carry = initial
    key_piece = lax.all_gather(key_pairs, "sp", axis=0, tiled=True)
    value_piece = lax.all_gather(value_pairs, "sp", axis=0, tiled=True)
    doc_piece = lax.all_gather(doc_pairs, "sp", axis=0, tiled=True)
    shards = key_piece.shape[0] * 2 // tok_rows
    joined = 1
    while joined * 2 <= shards and shards % (joined * 2) == 0 and (joined * 2 * tok_rows <= 1024):
        joined = joined * 2
    blocks = shards // joined
    span_rows = joined * tok_rows
    key_blocks = key_piece.reshape(blocks, span_rows, head_dim)
    value_blocks = value_piece.reshape(blocks, span_rows, head_dim)
    doc_blocks = doc_piece.reshape(blocks, span_rows)

    def visit(state, inputs):
        key_block, value_block, doc_block = inputs
        return (absorb_block(state, key_block, value_block, doc_block), None)

    carry, unused = lax.scan(visit, carry, (key_blocks, value_blocks, doc_blocks))
    attended = (carry[2] / carry[1][:, None]).astype(jnp.bfloat16)
    attended = (
        attended.reshape(local_heads, tok_rows, head_dim)
        .transpose(1, 0, 2)
        .reshape(tok_rows, local_heads * head_dim)
    )
    partial_value = jnp.dot(attended, out_weight, preferred_element_type=jnp.float32)
    mixed = lax.psum(
        partial_value.astype(jnp.bfloat16).astype(jnp.float32).astype(jnp.bfloat16), "tp"
    ).astype(jnp.float32)
    resid = tokens_in.astype(jnp.float32) + mixed
    normed = (
        resid * lax.rsqrt(jnp.mean(resid * resid, axis=-1, keepdims=True) + EPS) * norm_gain
    ).astype(jnp.bfloat16)
    gate = jnp.dot(
        normed,
        lax.all_gather(gate_weight, "sp", axis=0, tiled=True),
        preferred_element_type=jnp.float32,
    )
    up_val = jnp.dot(
        normed,
        lax.all_gather(up_weight, "sp", axis=0, tiled=True),
        preferred_element_type=jnp.float32,
    )
    hidden = (jax.nn.silu(gate) * up_val).astype(jnp.bfloat16)
    fed_part = jnp.dot(
        hidden,
        lax.all_gather(down_weight, "sp", axis=1, tiled=True),
        preferred_element_type=jnp.float32,
    )
    fed = lax.psum(
        fed_part.astype(jnp.bfloat16).astype(jnp.float32).astype(jnp.bfloat16), "tp"
    ).astype(jnp.float32)
    return (resid + fed).astype(jnp.bfloat16)


def solution(mesh):
    return jax.shard_map(
        per_device,
        mesh=mesh,
        in_specs=(
            P("sp", None),
            P("sp", "tp"),
            P("sp", "tp"),
            P("sp", "tp"),
            P("sp"),
            P(),
            P(),
            P("tp", None),
            P(),
            P("sp", "tp"),
            P("sp", "tp"),
            P("tp", "sp"),
        ),
        out_specs=P("sp", None),
        check_vma=False,
    )
```

profile of v0, /device:TPU:1, one launch (start us, length us, event | category | flops | bytes accessed | tf_op | source)
XLA Modules:
  0.0 459.8 jit_solution(11020853297494062564)
XLA Ops:
  7.4 1.4 fusion.48
  8.8 0.8 reshape.319
  9.6 1.0 copy.18
  10.7 0.7 fusion.22
  11.4 0.2 multiply_cosine_fusion.1
  11.7 0.2 copy.23
  11.9 0.8 fusion.23
  12.7 0.8 fusion.25
  13.5 0.2 fusion.39
  13.7 0.1 copy.17
  13.9 0.1 convert_element_type.69
  14.0 25.9 %all_gather.19 = bf16[1024,128]{1,0:T(8,128)(2,1)S(1)} all-gather(bf16[128,128]{1,0:T(8,128)(2,1)S(1)} %convert_element_type.69), channel_id=1, replica_groups=mesh['sp'=8,'tp'=4] {'sp'}, dimensions={0}, use_global_device_ids=true | all-gather | bytes 294912 | tf_op jit(solution)/shard_map/all_gather | solution.py:96
  39.9 0.2 reshape.321
  40.1 0.9 copy.20
  41.0 0.1 reshape.325
  41.1 24.7 %all_gather.20 = bf16[1024,128]{1,0:T(8,128)(2,1)S(1)} all-gather(bf16[128,128]{1,0:T(8,128)(2,1)S(1)} %reshape.325), channel_id=1, replica_groups=mesh['sp'=8,'tp'=4] {'sp'}, dimensions={0}, use_global_device_ids=true | all-gather | bytes 294912 | tf_op jit(solution)/shard_map/all_gather | solution.py:97
  65.8 0.2 reshape.326
  66.0 25.3 %all_gather.18 = s32[1024,2]{1,0:T(8,128)S(1)} all-gather(s32[128,2]{1,0:T(8,128)S(1)} %reshape.319), channel_id=1, replica_groups=mesh['sp'=8,'tp'=4] {'sp'}, dimensions={0}, use_global_device_ids=true | all-gather | bytes 9216 | tf_op jit(solution)/shard_map/all_gather | solution.py:98
  91.3 0.3 reshape.320
  91.7 9.8 %while.15 = (s32[]{:T(128)}, f32[1024]{0:T(1024)S(1)}, f32[1024]{0:T(1024)S(1)}, f32[1024,64]{0,1:T(8,128)S(1)}, s32[2,1024]{1,0:T(2,128)S(1)}, /*index=5*/s32[]...) while((s32[]{:T(128)}, f32[1024]{0:T(1024)S(1)}, ...), condition=%wide.region_7.8_spmd.clone, body=%wide.region_2.7_spmd.clone.sunk | while | flops 285345792 | bytes 14005583 | solution.py:113
  91.7 0.6 fusion.56
  94.8 3.6 conditional.3
  94.8 0.7 fusion.2
  95.6 1.5 fusion.4
  97.2 1.2 fusion.7
  98.4 0.6 fusion.56
  101.5 0.0 copy-start.1
  101.5 0.0 copy-start.4
  101.6 0.1 reshape.327
  101.7 1.4 convolution_convert_fusion
  103.1 0.0 all-reduce.3.cloned.1.call-update
  103.1 0.0 all-gather.4.cloned.1.call-start
  103.2 0.5 all-gather.4.cloned.1.call-update
  103.7 0.0 all-gather.6.cloned.1.call-start
  103.8 0.5 all-gather.6.cloned.1.call-update
  104.3 0.0 all-gather.8.cloned.1.call-start
  104.3 0.5 all-gather.8.cloned.1.call-update
  104.9 0.0 all-reduce.5.cloned.1.call-start
  104.9 56.8 %all-reduce.3.cloned.1.call-done = bf16[256,2048]{1,0:T(8,128)(2,1)} async-done(((bf16[256,2048]{1,0:T(8,128)(2,1)}), bf16[256,2048]{1,0:T(8,128)(2,1)}) %all-reduce.3.cloned.1.call-update) | async-done | bytes 1048592 | tf_op jit(solution)/shard_map/psum | solution.py:121
  161.7 1.7 multiply_reduce_fusion
  163.4 55.5 %all-gather.4.cloned.1.call-done = bf16[2048,1408]{1,0:T(8,128)(2,1)} async-done(((bf16[256,1408]{1,0:T(8,128)(2,1)}), bf16[2048,1408]{1,0:T(8,128)(2,1)}) %all-gather.4.cloned.1.call-update) | async-done | bytes 5767184 | tf_op jit(solution)/shard_map/all_gather | solution.py:130
  218.9 6.0 %fusion.46 = f32[256,1408]{1,0:T(8,128)} fusion(bf16[2048,1408]{1,0:T(8,128)(2,1)} %all-gather.4.cloned.1.call-done, bf16[256,2048]{1,0:T(8,128)(2,1)} %all-reduce.3.cloned.1.call-done, bf16[256,2048]{1,0:T(8,128)(2,1)S(1)} %copy-done.1, f32[2048]{0:T(1024)S(1)} %copy-done.4, f32[256]{0:T(256)S(1)} %add_rsqrt_fusion.1), kind=kOutput, calls=%fused_computation.86 | convolution fusion | flops 1479540736 | bytes 9315328 | tf_op jit(solution)/shard_map/dot_general | solution.py:128
  224.9 86.3 %all-gather.6.cloned.1.call-done = bf16[2048,1408]{1,0:T(8,128)(2,1)} async-done(((bf16[256,1408]{1,0:T(8,128)(2,1)}), bf16[2048,1408]{1,0:T(8,128)(2,1)}) %all-gather.6.cloned.1.call-update) | async-done | bytes 5767184 | tf_op jit(solution)/shard_map/all_gather | solution.py:135
  311.2 93.9 %all-gather.8.cloned.1.call-done = bf16[1408,2048]{1,0:T(8,128)(2,1)} async-done(((bf16[1408,256]{1,0:T(8,128)(2,1)}), bf16[1408,2048]{1,0:T(8,128)(2,1)}) %all-gather.8.cloned.1.call-update) | async-done | bytes 5767184 | tf_op jit(solution)/shard_map/all_gather | solution.py:141
  405.1 9.3 %convolution_convert_fusion.1 = bf16[256,2048]{1,0:T(8,128)(2,1)} fusion(bf16[1408,2048]{1,0:T(8,128)(2,1)} %all-gather.8.cloned.1.call-done, bf16[2048,1408]{1,0:T(8,128)(2,1)} %all-gather.6.cloned.1.call-done, f32[256,1408]{1,0:T(8,128)} %fusion.46, bf16[256,2048]{1,0:T(8,128)(2,1)S(1)} %copy-done.2, bf16[256,2048]{1,0:T(8,128)(2,1)S(1)} %copy-done.1, ...), kind=kOutput, calls=%fused_computation.26 | convolution fusion | flops 2958622720 | bytes 16131072 | tf_op jit(solution)/shard_map/dot_general | solution.py:139
  414.3 0.0 all-reduce.5.cloned.1.call-update
  414.4 35.1 %all-reduce.5.cloned.1.call-done = bf16[256,2048]{1,0:T(8,128)(2,1)} async-done(((bf16[256,2048]{1,0:T(8,128)(2,1)}), bf16[256,2048]{1,0:T(8,128)(2,1)}) %all-reduce.5.cloned.1.call-update) | async-done | bytes 1048592 | tf_op jit(solution)/shard_map/psum | solution.py:144
  449.5 2.7 add_convert_fusion
  (31 shorter events, 0.3 us)
Async XLA Ops:
  7.4 94.3 %copy-start = (bf16[256,2048]{1,0:T(8,128)(2,1)S(1)}, bf16[256,2048]{1,0:T(8,128)(2,1)}, u32[]{:S(2)}) copy-start(bf16[256,2048]{1,0:T(8,128)(2,1)} %param.23) | copy-start | bytes 3145732
  7.4 84.3 %copy-start.3 = (s32[256]{0:T(256)S(1)}, s32[256]{0:T(256)}, u32[]{:S(2)}) copy-start(s32[256]{0:T(256)} %param.20) | copy-start | bytes 3076
  7.4 154.3 %all-reduce.3.cloned.1.call-start = ((), (), s32[]{:S(2)}) async-start(), calls=%async_computation | async-start | bytes 2097152 | tf_op jit(solution)/shard_map/psum | solution.py:121
  101.5 60.2 %copy-start.1 = (bf16[256,2048]{1,0:T(8,128)(2,1)S(1)}, bf16[256,2048]{1,0:T(8,128)(2,1)}, u32[]{:S(2)}) copy-start(bf16[256,2048]{1,0:T(8,128)(2,1)} %param.16) | copy-start | bytes 3145732
  101.5 117.4 %copy-start.4 = (f32[2048]{0:T(1024)S(1)}, f32[2048]{0:T(1024)}, u32[]{:S(2)}) copy-start(f32[2048]{0:T(1024)} %param.24) | copy-start | bytes 24580
  103.1 115.7 %all-gather.4.cloned.1.call-start = ((), (), s32[]{:S(2)}) async-start(), calls=%async_computation.1 | async-start | bytes 6488064 | tf_op jit(solution)/shard_map/all_gather | solution.py:130
  103.7 207.5 %all-gather.6.cloned.1.call-start = ((), (), s32[]{:S(2)}) async-start(), calls=%async_computation.2 | async-start | bytes 6488064 | tf_op jit(solution)/shard_map/all_gather | solution.py:135
  104.3 300.8 %all-gather.8.cloned.1.call-start = ((), (), s32[]{:S(2)}) async-start(), calls=%async_computation.3 | async-start | bytes 6488064 | tf_op jit(solution)/shard_map/all_gather | solution.py:141
  104.9 344.6 %all-reduce.5.cloned.1.call-start = ((), (), s32[]{:S(2)}) async-start(), calls=%async_computation.4 | async-start | bytes 2097152 | tf_op jit(solution)/shard_map/psum | solution.py:144
  163.4 241.7 %copy-start.2 = (bf16[256,2048]{1,0:T(8,128)(2,1)S(1)}, bf16[256,2048]{1,0:T(8,128)(2,1)}, u32[]{:S(2)}) copy-start(bf16[256,2048]{1,0:T(8,128)(2,1)} %all-reduce.3.cloned.1.call-done) | copy-start | bytes 3145732
Sparse Core Ops, SparseCore 0:
  103.2 58.4 all-reduce.2
  414.5 34.9 all-reduce.4
Sparse Core Ops, SparseCore 1:
  105.8 113.0 all-gather.3
  220.9 90.2 all-gather.5
  313.1 91.9 all-gather.7
where the time goes:
time: 460 us
  waiting for transfers between devices  329 us (72%)
  blocking collectives  75.9 us (17%)
  matrix products  18.7 us (4%)
  between operations  15.2 us (3%)
  other arithmetic  8.87 us (2%)
  local copies, waits for them, and re-layouts  6.72 us (1%)
  loops' own time  5.06 us (1%)
    all_gather x1, waiting for transfers between devices, per_device(): lax.all_gather(down_weight, 'sp', axis=1, tiled=True)  93.9 us
    all_gather x1, waiting for transfers between devices, per_device(): lax.all_gather(up_weight, 'sp', axis=0, tiled=True)  86.3 us
    psum x1, waiting for transfers between devices, per_device(): lax.psum(partial_value.astype(jnp.bfloat16).astype(jnp.float32).astype(jn...  56.8 us
    all_gather x1, waiting for transfers between devices, per_device(): lax.all_gather(gate_weight, 'sp', axis=0, tiled=True)  55.5 us
    psum x1, waiting for transfers between devices, per_device(): lax.psum(fed_part.astype(jnp.bfloat16).astype(jnp.float32).astype(jnp.bfl...  35.1 us
    all_gather x1, blocking collectives, per_device(): key_piece = lax.all_gather(key_pairs, 'sp', axis=0, tiled=True)  25.9 us
    all_gather x1, blocking collectives, per_device(): doc_piece = lax.all_gather(doc_pairs, 'sp', axis=0, tiled=True)  25.3 us
    all_gather x1, blocking collectives, per_device(): value_piece = lax.all_gather(value_pairs, 'sp', axis=0, tiled=True)  24.7 us
  transfers between devices with their start and end apart: 5, of which 5 were waited for; matrix products, arithmetic and copies ran while one was open for 2% of the time, Pallas kernels for 0%

commit v1 on v0

--- a/solution.py
+++ b/solution.py
@@ -1,6 +1,10 @@
+import functools
+
 import jax
 import jax.numpy as jnp
 from jax import lax
+from jax.experimental import pallas as pl
+from jax.experimental.pallas import tpu as pltpu
 from jax.sharding import PartitionSpec as P
 
 GRID = 64
@@ -32,7 +36,240 @@
     return jnp.concatenate([by_row, by_col], axis=-1).astype(jnp.bfloat16)
 
 
+MESH = pl.DeviceIdType.MESH
+VM = pl.BlockSpec(memory_space=pltpu.VMEM)
+
+
+def params(cid):
+    return pltpu.CompilerParams(
+        collective_id=cid, has_side_effects=True, vmem_limit_bytes=56 * 1024 * 1024
+    )
+
+
+def greet(count, where):
+    barrier = pltpu.get_barrier_semaphore()
+
+    @pl.loop(1, count)
+    def _(step):
+        pl.semaphore_signal(barrier, inc=1, device_id=where(step), device_id_type=MESH)
+
+    pl.semaphore_wait(barrier, count - 1)
+
+
+def gather_kernel(n, kv_ref, doc_ref, kv_out, doc_out, send, recv, doc_send, doc_recv):
+    me = lax.axis_index("sp")
+
+    def where(step):
+        return {"sp": lax.rem(me + step, n)}
+
+    def copies(step, slot):
+        return (
+            pltpu.make_async_remote_copy(
+                kv_ref, kv_out.at[slot], send.at[step], recv.at[step], where(step), MESH
+            ),
+            pltpu.make_async_remote_copy(
+                doc_ref, doc_out.at[slot], doc_send.at[step], doc_recv.at[step], where(step), MESH
+            ),
+        )
+
+    greet(n, where)
+
+    @pl.loop(1, n)
+    def _(step):
+        for copy in copies(step, me):
+            copy.start()
+
+    kv_out[me] = kv_ref[...]
+    doc_out[me] = doc_ref[...]
+
+    @pl.loop(1, n)
+    def _(step):
+        for copy in copies(step, lax.rem(me + n - step, n)):
+            copy.wait_recv()
+            copy.wait_send()
+
+
+def gather_sp(n, packed, docs):
+    return pl.pallas_call(
+        functools.partial(gather_kernel, n),
+        out_shape=(
+            jax.ShapeDtypeStruct((n,) + packed.shape, packed.dtype),
+            jax.ShapeDtypeStruct((n,) + docs.shape, docs.dtype),
+        ),
+        in_specs=[VM, VM],
+        out_specs=(VM, VM),
+        scratch_shapes=[pltpu.SemaphoreType.DMA((n,))] * 4,
+        compiler_params=params(0),
+        name="gather_sp",
+    )(packed, docs)
+
+
+def mid_kernel(
+    nt, partial_ref, tokens_ref, gain_ref, normed_out, resid_out, landing, send, recv, send2, recv2
+):
+    sp, tp = lax.axis_index("sp"), lax.axis_index("tp")
+    side = lax.rem(sp, 2)
+    base = sp - side
+    group = 2 * nt
+    me = side * nt + tp
+    rows = resid_out.shape[0]
+
+    def where(step):
+        other = lax.rem(me + step, group)
+        return {"sp": base + other // nt, "tp": lax.rem(other, nt)}
+
+    def part(step):
+        peer = lax.rem(tp + step, nt)
+        return pltpu.make_async_remote_copy(
+            partial_ref.at[peer],
+            landing.at[step],
+            send.at[step],
+            recv.at[step],
+            {"sp": sp, "tp": peer},
+            MESH,
+        )
+
+    def spread(step, slot):
+        return pltpu.make_async_remote_copy(
+            normed_out.at[slot], normed_out.at[slot], send2.at[step], recv2.at[step], where(step), MESH
+        )
+
+    greet(group, where)
+    for step in range(1, nt):
+        part(step).start()
+    for step in range(1, nt):
+        part(step).wait_recv()
+    chunk = 16
+
+    @pl.loop(0, rows // chunk)
+    def _(i):
+        at = pl.ds(pl.multiple_of(i * chunk, chunk), chunk)
+        mixed = partial_ref[tp, at].astype(jnp.float32)
+        for step in range(1, nt):
+            mixed = mixed + landing[step, at].astype(jnp.float32)
+        resid = tokens_ref[tp, at].astype(jnp.float32) + mixed
+        resid_out[at] = resid
+        power = jnp.mean(resid * resid, axis=-1, keepdims=True)
+        normed_out[me, at] = (resid * lax.rsqrt(power + EPS) * gain_ref[...]).astype(jnp.bfloat16)
+
+    for step in range(1, group):
+        spread(step, me).start()
+    for step in range(1, group):
+        copy = spread(step, lax.rem(me + group - step, group))
+        copy.wait_recv()
+        copy.wait_send()
+    for step in range(1, nt):
+        part(step).wait_send()
+
+
+def mid_stage(nt, part, tokens, gain):
+    rows, width = part.shape[0] // nt, part.shape[1]
+    return pl.pallas_call(
+        functools.partial(mid_kernel, nt),
+        out_shape=(
+            jax.ShapeDtypeStruct((2 * nt, rows, width), jnp.bfloat16),
+            jax.ShapeDtypeStruct((rows, width), jnp.float32),
+        ),
+        in_specs=[VM, VM, VM],
+        out_specs=(VM, VM),
+        scratch_shapes=[pltpu.VMEM((nt, rows, width), jnp.bfloat16)]
+        + [pltpu.SemaphoreType.DMA((nt,))] * 2
+        + [pltpu.SemaphoreType.DMA((2 * nt,))] * 2,
+        compiler_params=params(1),
+        name="mid_stage",
+    )(part.reshape(nt, rows, width), tokens.reshape(nt, rows, width), gain.reshape(1, width))
+
+
+def last_kernel(nt, fed_ref, resid_ref, out_ref, landing, send, recv, send2, recv2):
+    sp, tp = lax.axis_index("sp"), lax.axis_index("tp")
+    side = lax.rem(sp, 2)
+    base = sp - side
+    group = 2 * nt
+    me = side * nt + tp
+    rows = resid_ref.shape[0]
+
+    def where(step):
+        other = lax.rem(me + step, group)
+        return {"sp": base + other // nt, "tp": lax.rem(other, nt)}
+
+    def part(step):
+        return pltpu.make_async_remote_copy(
+            fed_ref.at[lax.rem(me + step, group)],
+            landing.at[step],
+            send.at[step],
+            recv.at[step],
+            where(step),
+            MESH,
+        )
+
+    def spread(step, slot):
+        return pltpu.make_async_remote_copy(
+            out_ref.at[slot],
+            out_ref.at[slot],
+            send2.at[step],
+            recv2.at[step],
+            {"sp": sp, "tp": lax.rem(tp + step, nt)},
+            MESH,
+        )
+
+    greet(group, where)
+    for step in range(1, group):
+        part(step).start()
+    for step in range(1, group):
+        part(step).wait_recv()
+    chunk = 16
+
+    @pl.loop(0, rows // chunk)
+    def _(i):
+        at = pl.ds(pl.multiple_of(i * chunk, chunk), chunk)
+        fed = fed_ref[me, at].astype(jnp.float32)
+        for step in range(1, group):
+            fed = fed + landing[step, at].astype(jnp.float32)
+        out_ref[tp, at] = (resid_ref[at] + fed).astype(jnp.bfloat16)
+
+    for step in range(1, nt):
+        spread(step, tp).start()
+    for step in range(1, nt):
+        copy = spread(step, lax.rem(tp + nt - step, nt))
+        copy.wait_recv()
+        copy.wait_send()
+    for step in range(1, group):
+        part(step).wait_send()
+
+
+def last_stage(nt, fed, resid):
+    rows, width = resid.shape
+    return pl.pallas_call(
+        functools.partial(last_kernel, nt),
+        out_shape=jax.ShapeDtypeStruct((nt, rows, width), jnp.bfloat16),
+        in_specs=[VM, VM],
+        out_specs=VM,
+        scratch_shapes=[pltpu.VMEM((2 * nt, rows, width), jnp.bfloat16)]
+        + [pltpu.SemaphoreType.DMA((2 * nt,))] * 2
+        + [pltpu.SemaphoreType.DMA((nt,))] * 2,
+        compiler_params=params(2),
+        name="last_stage",
+    )(fed.reshape(2 * nt, rows, width), resid)
+
+
+def pair_share(n, arrays, axis, joins):
+    side = lax.rem(lax.axis_index("sp"), 2)
+    own, away = [], []
+    for array in arrays:
+        half = array.shape[axis] // 2
+        own.append(lax.dynamic_slice_in_dim(array, side * half, half, axis))
+        away.append(lax.dynamic_slice_in_dim(array, (1 - side) * half, half, axis))
+    own = jnp.concatenate(own, axis=axis)
+    away = jnp.concatenate(away, axis=axis)
+    came = lax.ppermute(away, "sp", [(i, i ^ 1) for i in range(n)])
+    first = jnp.where(side == 0, own, came)
+    second = jnp.where(side == 0, came, own)
+    return jnp.concatenate([first, second], axis=joins)
+
+
 def per_device(
+    n,
+    nt,
     tokens_in,
     queries,
     keys,
@@ -54,11 +291,16 @@
     lattice_column = (places % GRID).astype(jnp.float32)
     q_local = normalized_rotated(queries, query_gain, local_heads, lattice_row, lattice_column)
     q_rows = q_local.transpose(1, 0, 2).reshape(local_heads * tok_rows, head_dim)
-    key_pairs = normalized_rotated(keys, key_norm_scale, 1, lattice_row, lattice_column).reshape(
-        tok_rows // 2, 2 * head_dim
-    )
-    value_pairs = values.reshape(tok_rows // 2, 2 * head_dim)
-    doc_pairs = doc_ids.reshape(tok_rows // 2, 2)
+    lanes = [[2 * j + side for j in range(n // 2)] for side in range(2)]
+    gate_up_all = lax.all_gather(
+        pair_share(n, [gate_weight, up_weight], 1, 0), "sp", axis_index_groups=lanes, axis=0, tiled=True
+    )
+    down_all = lax.all_gather(
+        pair_share(n, [down_weight], 0, 1), "sp", axis_index_groups=lanes, axis=1, tiled=True
+    )
+    turned = normalized_rotated(keys, key_norm_scale, 1, lattice_row, lattice_column)
+    packed = jnp.concatenate([turned.reshape(tok_rows, head_dim), values], axis=1)
+    kv_all, doc_all = gather_sp(n, packed, doc_ids.reshape(1, tok_rows))
     row_docs = jnp.tile(doc_ids, local_heads)
     first_doc = doc_ids[0]
     last_doc = doc_ids[-1]
@@ -93,18 +335,15 @@
         jnp.zeros((total_rows, head_dim), jnp.float32),
     )
     carry = initial
-    key_piece = lax.all_gather(key_pairs, "sp", axis=0, tiled=True)
-    value_piece = lax.all_gather(value_pairs, "sp", axis=0, tiled=True)
-    doc_piece = lax.all_gather(doc_pairs, "sp", axis=0, tiled=True)
-    shards = key_piece.shape[0] * 2 // tok_rows
+    shards = n
     joined = 1
     while joined * 2 <= shards and shards % (joined * 2) == 0 and (joined * 2 * tok_rows <= 1024):
         joined = joined * 2
     blocks = shards // joined
     span_rows = joined * tok_rows
-    key_blocks = key_piece.reshape(blocks, span_rows, head_dim)
-    value_blocks = value_piece.reshape(blocks, span_rows, head_dim)
-    doc_blocks = doc_piece.reshape(blocks, span_rows)
+    key_blocks = kv_all[..., :head_dim].reshape(blocks, span_rows, head_dim)
+    value_blocks = kv_all[..., head_dim:].reshape(blocks, span_rows, head_dim)
+    doc_blocks = doc_all.reshape(blocks, span_rows)
 
     def visit(state, inputs):
         key_block, value_block, doc_block = inputs
@@ -118,38 +357,19 @@
         .reshape(tok_rows, local_heads * head_dim)
     )
     partial_value = jnp.dot(attended, out_weight, preferred_element_type=jnp.float32)
-    mixed = lax.psum(
-        partial_value.astype(jnp.bfloat16).astype(jnp.float32).astype(jnp.bfloat16), "tp"
-    ).astype(jnp.float32)
-    resid = tokens_in.astype(jnp.float32) + mixed
-    normed = (
-        resid * lax.rsqrt(jnp.mean(resid * resid, axis=-1, keepdims=True) + EPS) * norm_gain
-    ).astype(jnp.bfloat16)
-    gate = jnp.dot(
-        normed,
-        lax.all_gather(gate_weight, "sp", axis=0, tiled=True),
-        preferred_element_type=jnp.float32,
-    )
-    up_val = jnp.dot(
-        normed,
-        lax.all_gather(up_weight, "sp", axis=0, tiled=True),
-        preferred_element_type=jnp.float32,
-    )
-    hidden = (jax.nn.silu(gate) * up_val).astype(jnp.bfloat16)
-    fed_part = jnp.dot(
-        hidden,
-        lax.all_gather(down_weight, "sp", axis=1, tiled=True),
-        preferred_element_type=jnp.float32,
-    )
-    fed = lax.psum(
-        fed_part.astype(jnp.bfloat16).astype(jnp.float32).astype(jnp.bfloat16), "tp"
-    ).astype(jnp.float32)
-    return (resid + fed).astype(jnp.bfloat16)
+    normed, resid = mid_stage(nt, partial_value.astype(jnp.bfloat16), tokens_in, norm_gain)
+    normed = normed.reshape(2 * tok_rows, -1)
+    both = jnp.dot(normed, gate_up_all, preferred_element_type=jnp.float32)
+    units = both.shape[1] // 2
+    hidden = (jax.nn.silu(both[:, :units]) * both[:, units:]).astype(jnp.bfloat16)
+    fed_part = jnp.dot(hidden, down_all, preferred_element_type=jnp.float32)
+    out = last_stage(nt, fed_part.astype(jnp.bfloat16), resid)
+    return out.reshape(tok_rows, -1)
 
 
 def solution(mesh):
     return jax.shard_map(
-        per_device,
+        functools.partial(per_device, mesh.shape["sp"], mesh.shape["tp"]),
         mesh=mesh,
         in_specs=(
             P("sp", None),

time: 460 us -> 264 us (0.57)
  waiting for transfers between devices: 329 us -> 101 us
  Pallas kernels: 0 us -> 106 us
  blocking collectives: 75.9 us -> 0 us
    all_gather x3 -> x2, waiting for transfers between devices: 236 us -> 77.3 us  [the longest x1 50.4 us: per_device(): lax.all_gather(pair_share(n, [down_weight], 0, 1), 'sp', axis_index_group...]
    pallas_call x0 -> x3, Pallas kernels: none -> 106 us  [the longest x1 43 us: mid_stage(): pl.pallas_call(functools.partial(mid_kernel, nt), out_shape=(jax.ShapeDty...]
    psum x2 -> x0, waiting for transfers between devices: 91.9 us -> none  [the longest x1 56.8 us: per_device(): lax.psum(partial_value.astype(jnp.bfloat16).astype(jnp.float32).astype(jn...]
    all_gather x3 -> x0, blocking collectives: 75.9 us -> none  [the longest x1 25.9 us: per_device(): key_piece = lax.all_gather(key_pairs, 'sp', axis=0, tiled=True)]
    ppermute x0 -> x2, waiting for transfers between devices: none -> 23.4 us  [pair_share(): came = lax.ppermute(away, 'sp', [(i, i ^ 1) for i in range(n)])]
  transfers between devices with their start and end apart: 5 -> 4, of which waited for: 5 -> 4; matrix products, arithmetic and copies ran while one was open for 2% -> 8% of each run, Pallas kernels for 0% -> 25%
where the time goes in v1:
time: 264 us; the launch traced here: 263 us
  Pallas kernels  106 us (40%)
  waiting for transfers between devices  101 us (38%)
  matrix products  17.6 us (7%)
  between operations  13.7 us (5%)
  local copies, waits for them, and re-layouts  9.25 us (4%)
  other arithmetic  7.09 us (3%)
  loops' own time  5.05 us (2%)
  starting transfers between devices  3.41 us (1%)
    all_gather x1, waiting for transfers between devices, per_device(): lax.all_gather(pair_share(n, [down_weight], 0, 1), 'sp', axis_index_group...  50.4 us
    pallas_call x1, Pallas kernels, mid_stage(): pl.pallas_call(functools.partial(mid_kernel, nt), out_shape=(jax.ShapeDty...  43 us
    pallas_call x1, Pallas kernels, last_stage(): pl.pallas_call(functools.partial(last_kernel, nt), out_shape=jax.ShapeDty...  40.7 us
    all_gather x1, waiting for transfers between devices, per_device(): lax.all_gather(pair_share(n, [gate_weight, up_weight], 1, 0), 'sp', axis_...  26.9 us
    ppermute x2, waiting for transfers between devices, pair_share(): came = lax.ppermute(away, 'sp', [(i, i ^ 1) for i in range(n)])  23.4 us
    pallas_call x1, Pallas kernels, gather_sp(): pl.pallas_call(functools.partial(gather_kernel, n), out_shape=(jax.ShapeD...  22.7 us
    dot_general x1, matrix products, per_device(): both = jnp.dot(normed, gate_up_all, preferred_element_type=jnp.float32)  8.29 us
    dot_general x1, matrix products, per_device(): fed_part = jnp.dot(hidden, down_all, preferred_element_type=jnp.float32)  5.96 us
  transfers between devices with their start and end apart: 4, of which 4 were waited for; matrix products, arithmetic and copies ran while one was open for 8% of the time, Pallas kernels for 25%

profile of v1, /device:TPU:1, one launch (start us, length us, event | category | flops | bytes accessed | tf_op | source)
XLA Modules:
  0.0 263.3 jit_solution(7590346824540702344)
XLA Ops:
  6.5 2.2 constant_dynamic-slice_fusion.5
  8.8 0.2 pad_maximum_fusion.2
  9.0 2.1 collective-permute-start
  11.1 15.8 %collective-permute-done = bf16[256,1408]{1,0:T(8,128)(2,1)S(1)} collective-permute-done((bf16[256,1408]{1,0:T(8,128)(2,1)S(1)}, bf16[256,1408]{1,0:T(8,128)(2,1)S(1)}, u32[]{:S(2)}, u32[]{:S(2)}) %collective-permute-start) | collective-permute-done | bytes 720928 | tf_op jit(solution)/shard_map/ppermute | solution.py:264
  26.9 0.4 broadcast_select_fusion.1
  27.3 0.0 copy-start.1
  27.3 1.2 pad_maximum_fusion
  28.6 0.0 all-gather.3.cloned.1.call-update
  28.6 0.0 all-gather.5.cloned.1.call-start
  28.7 0.0 copy-start.4
  28.7 0.0 copy-start.5
  28.7 0.0 copy-start.7
  28.7 1.2 collective-permute-start.1
  30.0 7.5 %collective-permute-done.1 = bf16[704,256]{1,0:T(8,128)(2,1)S(1)} collective-permute-done((bf16[704,256]{1,0:T(8,128)(2,1)S(1)}, bf16[704,256]{1,0:T(8,128)(2,1)S(1)}, u32[]{:S(2)}, u32[]{:S(2)}) %collective-permute-start.1) | collective-permute-done | bytes 360480 | tf_op jit(solution)/shard_map/ppermute | solution.py:264
  37.5 0.2 broadcast_select_fusion.3
  37.7 0.0 copy-start.3
  37.7 0.9 pad_maximum_fusion.3
  38.7 0.0 all-gather.5.cloned.1.call-update
  38.7 0.1 copy.29
  38.9 0.2 multiply_cosine_fusion.3
  39.1 0.1 fusion.24
  39.3 0.2 copy.33
  39.5 0.1 copy.25
  39.6 0.1 copy.28
  39.7 0.1 fusion.33
  39.8 0.1 fusion.35
  39.9 1.2 fusion.46
  41.2 0.8 concatenate.37.kv_ref
  42.0 22.7 %gather_sp.1 = (bf16[8,256,128]{2,1,0:T(8,128)(2,1)}, s32[8,1,256]{2,1,0:T(1,128)}) custom-call(bf16[256,128]{1,0:T(8,128)(2,1)} %concatenate.37.kv_ref, s32[1,256]{1,0:T(1,128)S(1)} %bitcast.84), custom_call_target="tpu_custom_call" | custom-call | tf_op jit(solution)/shard_map/gather_sp/pallas_call | solution.py:93
  64.7 0.7 reduce.2
  65.4 0.6 fusion.54
  66.0 1.4 fusion.53
  67.5 9.8 %while.15 = (s32[]{:T(128)}, f32[1024]{0:T(1024)S(1)}, f32[1024]{0:T(1024)S(1)}, f32[1024,64]{0,1:T(8,128)S(1)}, s32[2,1024]{1,0:T(2,128)S(1)}, /*index=5*/s32[]...) while((s32[]{:T(128)}, f32[1024]{0:T(1024)S(1)}, ...), condition=%wide.region_7.8_spmd.clone, body=%wide.region_2.7_spmd.clone.sunk | while | flops 285345792 | bytes 14005583 | solution.py:352
  67.6 0.6 fusion.63
  70.6 3.6 %conditional.3 = ((f32[1024]{0:T(1024)S(1)}, f32[1024]{0:T(1024)S(1)}, f32[1024,64]{0,1:T(8,128)S(1)})) conditional(s32[]{:T(128)} %convert_element_type.71, (f32[1024]{0:T(1024)S(1)}, f32[1024]{0:T(1024)S(1)}, f32[1024,64]{0,1:T(8,128)S(1)}) %tuple.64, (s32[256]{0:T(256)S(1)}, s32[1,1024]{1,0:T(1,128)S(1)}, bf16[2,1024,64]{2,1,0:T(8,128)(2,1)S(1)}, ...), branch_computations={%region_3.3_spmd, %region_4.6_spmd} | conditional | flops 285345792 | bytes 13997096 | solution.py:330
  70.6 0.7 fusion.2
  71.4 1.5 fusion.4
  73.0 1.2 fusion.7
  74.2 0.6 fusion.63
  77.3 0.1 reshape.342
  77.4 1.4 convolution_convert_fusion.1
  78.9 43.0 %mid_stage.1 = (bf16[8,64,2048]{2,1,0:T(8,128)(2,1)}, f32[64,2048]{1,0:T(8,128)}) custom-call(bf16[4,64,2048]{2,1,0:T(8,128)(2,1)} %bitcast.70, bf16[4,64,2048]{2,1,0:T(8,128)(2,1)} %bitcast.72, f32[1,2048]{1,0:T(1,128)} %bitcast.85), custom_call_target="tpu_custom_call" | custom-call | tf_op jit(solution)/shard_map/mid_stage/pallas_call | solution.py:167
  121.9 26.9 %all-gather.3.cloned.1.call-done = bf16[2048,1408]{1,0:T(8,128)(2,1)} async-done(((bf16[512,1408]{1,0:T(8,128)(2,1)}), bf16[2048,1408]{1,0:T(8,128)(2,1)}) %all-gather.3.cloned.1.call-update) | async-done | bytes 5767184 | tf_op jit(solution)/shard_map/all_gather | solution.py:295
  148.8 8.3 %fusion.55 = f32[512,1408]{1,0:T(8,128)} fusion(bf16[512,2048]{1,0:T(8,128)(2,1)} %bitcast.86, bf16[2048,1408]{1,0:T(8,128)(2,1)} %all-gather.3.cloned.1.call-done), kind=kOutput, calls=%fused_computation.101 | convolution fusion | flops 2952790016 | bytes 10747904 | tf_op jit(solution)/shard_map/dot_general | solution.py:362
  157.1 50.4 %all-gather.5.cloned.1.call-done = bf16[704,2048]{1,0:T(8,128)(2,1)} async-done(((bf16[704,512]{1,0:T(8,128)(2,1)}), bf16[704,2048]{1,0:T(8,128)(2,1)}) %all-gather.5.cloned.1.call-update) | async-done | bytes 2883600 | tf_op jit(solution)/shard_map/all_gather | solution.py:298
  207.5 6.0 %convolution_convert_fusion = bf16[512,2048]{1,0:T(8,128)(2,1)} fusion(bf16[704,2048]{1,0:T(8,128)(2,1)} %all-gather.5.cloned.1.call-done, f32[512,1408]{1,0:T(8,128)} %fusion.55), kind=kOutput, calls=%fused_computation.23 | convolution fusion | flops 1479606272 | bytes 8126464 | tf_op jit(solution)/shard_map/dot_general | solution.py:365
  213.5 40.7 %last_stage.1 = bf16[4,64,2048]{2,1,0:T(8,128)(2,1)} custom-call(bf16[8,64,2048]{2,1,0:T(8,128)(2,1)} %bitcast.71, f32[64,2048]{1,0:T(8,128)} %get-tuple-element.156.resid_ref), custom_call_target="tpu_custom_call" | custom-call | tf_op jit(solution)/shard_map/last_stage/pallas_call | solution.py:242
  254.2 2.3 copy.55
  (34 shorter events, 0.3 us)
Async XLA Ops:
  6.5 70.9 %copy-start = (bf16[256,2048]{1,0:T(8,128)(2,1)S(1)}, bf16[256,2048]{1,0:T(8,128)(2,1)}, u32[]{:S(2)}) copy-start(bf16[256,2048]{1,0:T(8,128)(2,1)} %param.23) | copy-start | bytes 3145732
  6.5 142.3 %all-gather.3.cloned.1.call-start = ((), (), s32[]{:S(2)}) async-start(), calls=%async_computation | async-start | bytes 7208960 | tf_op jit(solution)/shard_map/all_gather | solution.py:295
  9.0 18.0 %collective-permute-start = (bf16[256,1408]{1,0:T(8,128)(2,1)S(1)}, bf16[256,1408]{1,0:T(8,128)(2,1)S(1)}, u32[]{:S(2)}, u32[]{:S(2)}) collective-permute-start(bf16[256,1408]{1,0:T(8,128)(2,1)S(1)} %pad_maximum_fusion.2), channel_id=1, source_target_pairs={{0,4},{4,0},{8,12},{12,8},{16,20},{20,16},{24,28},{28,24},{1,5},{5... | collective-permute-start | bytes 2162696 | tf_op jit(solution)/shard_map/ppermute | solution.py:264
  27.3 1.3 copy-start.1
  28.6 10.1 %copy-start.2 = (bf16[256,256]{1,0:T(8,128)(2,1)S(1)}, bf16[256,256]{1,0:T(8,128)(2,1)}, u32[]{:S(2)}) copy-start(bf16[256,256]{1,0:T(8,128)(2,1)} %param.17) | copy-start | bytes 393220
  28.6 10.5 %copy-start.6 = (f32[64]{0:T(128)S(1)}, f32[64]{0:T(128)}, u32[]{:S(2)}) copy-start(f32[64]{0:T(128)} %param.21) | copy-start | bytes 772
  28.6 178.9 %all-gather.5.cloned.1.call-start = ((), (), s32[]{:S(2)}) async-start(), calls=%async_computation.1 | async-start | bytes 3604480 | tf_op jit(solution)/shard_map/all_gather | solution.py:298
  28.7 10.7 %copy-start.4 = (bf16[256,64]{0,1:T(8,128)(2,1)S(1)}, bf16[256,64]{0,1:T(8,128)(2,1)}, u32[]{:S(2)}) copy-start(bf16[256,64]{0,1:T(8,128)(2,1)} %param.18) | copy-start | bytes 98308
  28.7 10.9 %copy-start.5 = (bf16[256,64]{0,1:T(8,128)(2,1)S(1)}, bf16[256,64]{0,1:T(8,128)(2,1)}, u32[]{:S(2)}) copy-start(bf16[256,64]{0,1:T(8,128)(2,1)} %param.19) | copy-start | bytes 98308
  28.7 11.1 %copy-start.7 = (f32[64]{0:T(128)S(1)}, f32[64]{0:T(128)}, u32[]{:S(2)}) copy-start(f32[64]{0:T(128)} %param.22) | copy-start | bytes 772
  28.7 8.8 %collective-permute-start.1 = (bf16[704,256]{1,0:T(8,128)(2,1)S(1)}, bf16[704,256]{1,0:T(8,128)(2,1)S(1)}, u32[]{:S(2)}, u32[]{:S(2)}) collective-permute-start(bf16[704,256]{1,0:T(8,128)(2,1)S(1)} %constant_dynamic-slice_fusion.2), channel_id=1, source_target_pairs={{0,4},{4,0},{8,12},{12,8},{16,20},{20,16},{24,28},{28,24},{1,5},{5... | collective-permute-start | bytes 1081352 | tf_op jit(solution)/shard_map/ppermute | solution.py:264
  37.7 4.2 %copy-start.3 = (s32[256]{0:T(256)S(1)}, s32[256]{0:T(256)}, u32[]{:S(2)}) copy-start(s32[256]{0:T(256)} %param.20) | copy-start | bytes 3076
Sparse Core Ops, SparseCore 0:
  28.7 120.0 all-gather.2
  150.4 57.0 all-gather.4

commit v2 on v1

--- a/solution.py
+++ b/solution.py
@@ -295,9 +295,17 @@
     gate_up_all = lax.all_gather(
         pair_share(n, [gate_weight, up_weight], 1, 0), "sp", axis_index_groups=lanes, axis=0, tiled=True
     )
-    down_all = lax.all_gather(
-        pair_share(n, [down_weight], 0, 1), "sp", axis_index_groups=lanes, axis=1, tiled=True
-    )
+    down_pair = pair_share(n, [down_weight], 0, 1)
+    lane, count = lax.axis_index("sp") // 2, n // 2
+    span = down_pair.shape[1]
+    down_all = jnp.zeros((down_pair.shape[0], count * span), down_pair.dtype)
+    for shift in range(count):
+        piece = down_pair
+        if shift:
+            piece = lax.ppermute(down_pair, "sp", [(i, (i + 2 * shift) % n) for i in range(n)])
+        down_all = lax.dynamic_update_slice_in_dim(
+            down_all, piece, lax.rem(lane + count - shift, count) * span, 1
+        )
     turned = normalized_rotated(keys, key_norm_scale, 1, lattice_row, lattice_column)
     packed = jnp.concatenate([turned.reshape(tok_rows, head_dim), values], axis=1)
     kv_all, doc_all = gather_sp(n, packed, doc_ids.reshape(1, tok_rows))

time: 264 us -> 267 us (1.011)
  waiting for transfers between devices: 101 us -> 79.9 us
  starting transfers between devices: 3.41 us -> 14.1 us
  local copies, waits for them, and re-layouts: 9.25 us -> 17.8 us
    all_gather x1 -> x0, waiting for transfers between devices: 50.4 us -> none  [per_device(): lax.all_gather(pair_share(n, [down_weight], 0, 1), 'sp', axis_index_group...]
    ppermute x0 -> x3, waiting for transfers between devices: none -> 23.1 us  [per_device(): lax.ppermute(down_pair, 'sp', [(i, (i + 2 * shift) % n) for i in range(n)])]
    all_gather x1, waiting for transfers between devices: 26.9 us -> 40.9 us  [per_device(): lax.all_gather(pair_share(n, [gate_weight, up_weight], 1, 0), 'sp', axis_...]
    ppermute x0 -> x3, starting transfers between devices: none -> 10.7 us  [per_device(): lax.ppermute(down_pair, 'sp', [(i, (i + 2 * shift) % n) for i in range(n)])]
    ppermute x2, waiting for transfers between devices: 23.4 us -> 15.8 us  [pair_share(): came = lax.ppermute(away, 'sp', [(i, i ^ 1) for i in range(n)])]
    pallas_call x1, Pallas kernels: 43 us -> 48.1 us  [mid_stage(): pl.pallas_call(functools.partial(mid_kernel, nt), out_shape=(jax.ShapeDty...]
    dynamic_update_slice x0 -> x3, local copies, waits for them, and re-layouts: none -> 4.05 us  [per_device(): lax.dynamic_update_slice_in_dim(down_all, piece, lax.rem(lane + count - s...]
    pallas_call x1, Pallas kernels: 22.7 us -> 19.4 us  [gather_sp(): pl.pallas_call(functools.partial(gather_kernel, n), out_shape=(jax.ShapeD...]
  transfers between devices with their start and end apart: 4 -> 6, of which waited for: 4 -> 4; matrix products, arithmetic and copies ran while one was open for 8% -> 11% of each run, Pallas kernels for 25% -> 25%
where the time goes in v2:
time: 267 us
  Pallas kernels  108 us (40%)
  waiting for transfers between devices  79.9 us (30%)
  matrix products  18.8 us (7%)
  local copies, waits for them, and re-layouts  17.8 us (7%)
  starting transfers between devices  14.1 us (5%)
  between operations  13.8 us (5%)
  other arithmetic  9.35 us (4%)
  loops' own time  5.11 us (2%)
    pallas_call x1, Pallas kernels, mid_stage(): pl.pallas_call(functools.partial(mid_kernel, nt), out_shape=(jax.ShapeDty...  48.1 us
    all_gather x1, waiting for transfers between devices, per_device(): lax.all_gather(pair_share(n, [gate_weight, up_weight], 1, 0), 'sp', axis_...  40.9 us
    pallas_call x1, Pallas kernels, last_stage(): pl.pallas_call(functools.partial(last_kernel, nt), out_shape=jax.ShapeDty...  40.4 us
    ppermute x3, waiting for transfers between devices, per_device(): lax.ppermute(down_pair, 'sp', [(i, (i + 2 * shift) % n) for i in range(n)])  23.1 us
    pallas_call x1, Pallas kernels, gather_sp(): pl.pallas_call(functools.partial(gather_kernel, n), out_shape=(jax.ShapeD...  19.4 us
    ppermute x2, waiting for transfers between devices, pair_share(): came = lax.ppermute(away, 'sp', [(i, i ^ 1) for i in range(n)])  15.8 us
    ppermute x3, starting transfers between devices, per_device(): lax.ppermute(down_pair, 'sp', [(i, (i + 2 * shift) % n) for i in range(n)])  10.7 us
    dot_general x1, matrix products, per_device(): both = jnp.dot(normed, gate_up_all, preferred_element_type=jnp.float32)  6.38 us
  transfers between devices with their start and end apart: 6, of which 4 were waited for; matrix products, arithmetic and copies ran while one was open for 11% of the time, Pallas kernels for 25%

profile of v2, /device:TPU:1, one launch (start us, length us, event | category | flops | bytes accessed | tf_op | source)
XLA Modules:
  0.0 266.6 jit_solution(12165358161256793005)
XLA Ops:
  6.5 2.2 constant_dynamic-slice_fusion.5
  8.8 0.2 pad_maximum_fusion.2
  9.0 2.1 collective-permute-start
  11.1 15.8 %collective-permute-done = bf16[256,1408]{1,0:T(8,128)(2,1)S(1)} collective-permute-done((bf16[256,1408]{1,0:T(8,128)(2,1)S(1)}, bf16[256,1408]{1,0:T(8,128)(2,1)S(1)}, u32[]{:S(2)}, u32[]{:S(2)}) %collective-permute-start) | collective-permute-done | bytes 720928 | tf_op jit(solution)/shard_map/ppermute | solution.py:264
  26.9 0.4 broadcast_select_fusion.1
  27.4 1.2 pad_maximum_fusion
  28.7 1.2 collective-permute-start.1
  30.1 0.2 multiply_cosine_fusion.3
  30.5 0.8 copy.33
  31.3 0.1 copy.25
  31.5 0.1 copy.28
  31.6 0.1 fusion.33
  31.8 1.2 fusion.46
  33.0 0.8 concatenate.37.kv_ref
  33.8 19.4 %gather_sp.1 = (bf16[8,256,128]{2,1,0:T(8,128)(2,1)}, s32[8,1,256]{2,1,0:T(1,128)}) custom-call(bf16[256,128]{1,0:T(8,128)(2,1)} %concatenate.37.kv_ref, s32[1,256]{1,0:T(1,128)S(1)} %bitcast.84), custom_call_target="tpu_custom_call" | custom-call | tf_op jit(solution)/shard_map/gather_sp/pallas_call | solution.py:93
  53.2 0.7 reduce.2
  54.0 0.6 fusion.54
  54.6 2.4 fusion.53
  56.9 0.2 broadcast_select_fusion.3
  57.1 2.0 broadcast_in_dim.21
  59.1 1.0 pad_maximum_fusion.3
  60.1 9.9 %collective-permute-start.2 = (bf16[704,512]{1,0:T(8,128)(2,1)S(1)}, bf16[704,512]{1,0:T(8,128)(2,1)S(1)}, u32[]{:S(2)}, u32[]{:S(2)}) collective-permute-start(bf16[704,512]{1,0:T(8,128)(2,1)S(1)} %get-tuple-element.244), channel_id=1, source_target_pairs={{0,8},{4,12},{8,16},{12,20},{16,24},{20,28},{24,0},{28,4},{1,9},{5... | collective-permute-start | bytes 2162696 | tf_op jit(solution)/shard_map/ppermute | solution.py:305
  70.0 0.8 collective-permute-start.3
  70.8 15.4 %while.15 = (s32[]{:T(128)}, f32[1024]{0:T(1024)S(1)}, f32[1024]{0:T(1024)S(1)}, f32[1024,64]{0,1:T(8,128)S(1)}, s32[2,1024]{1,0:T(2,128)S(1)}, /*index=5*/s32[]...) while((s32[]{:T(128)}, f32[1024]{0:T(1024)S(1)}, ...), condition=%wide.region_7.8_spmd.clone, body=%wide.region_2.7_spmd.clone.sunk | while | flops 285345792 | bytes 15054695 | solution.py:360
  70.8 0.6 fusion.63
  73.9 4.6 %conditional.3 = ((f32[1024]{0:T(1024)S(1)}, f32[1024]{0:T(1024)S(1)}, f32[1024,64]{0,1:T(8,128)S(1)})) conditional(s32[]{:T(128)} %convert_element_type.71, (f32[1024]{0:T(1024)S(1)}, f32[1024]{0:T(1024)S(1)}, f32[1024,64]{0,1:T(8,128)S(1)}) %tuple.65, (s32[256]{0:T(256)S(1)}, s32[1,1024]{1,0:T(1,128)S(1)}, bf16[2,1024,64]{2,1,0:T(8,128)(2,1)}, ...), branch_computations={%region_3.3_spmd, %region_4.6_spmd} | conditional | flops 285345792 | bytes 15046208 | solution.py:338
  73.9 1.8 fusion.2
  75.7 1.5 fusion.4
  77.3 1.2 fusion.7
  78.6 0.6 fusion.63
  81.6 4.6 %conditional.3 = ((f32[1024]{0:T(1024)S(1)}, f32[1024]{0:T(1024)S(1)}, f32[1024,64]{0,1:T(8,128)S(1)})) conditional(s32[]{:T(128)} %convert_element_type.71, (f32[1024]{0:T(1024)S(1)}, f32[1024]{0:T(1024)S(1)}, f32[1024,64]{0,1:T(8,128)S(1)}) %tuple.65, (s32[256]{0:T(256)S(1)}, s32[1,1024]{1,0:T(1,128)S(1)}, bf16[2,1024,64]{2,1,0:T(8,128)(2,1)}, ...), branch_computations={%region_3.3_spmd, %region_4.6_spmd} | conditional | flops 285345792 | bytes 15046208 | solution.py:338
  81.6 1.8 fusion.2
  83.4 1.5 fusion.4
  85.0 1.2 fusion.7
  86.4 0.7 divide_convert_fusion
  87.0 1.0 reshape.342
  88.1 1.4 convolution_convert_fusion.1
  89.5 48.1 %mid_stage.1 = (bf16[8,64,2048]{2,1,0:T(8,128)(2,1)}, f32[64,2048]{1,0:T(8,128)}) custom-call(bf16[4,64,2048]{2,1,0:T(8,128)(2,1)} %bitcast.70, bf16[4,64,2048]{2,1,0:T(8,128)(2,1)} %bitcast.72, f32[1,2048]{1,0:T(1,128)} %bitcast.85), custom_call_target="tpu_custom_call" | custom-call | tf_op jit(solution)/shard_map/mid_stage/pallas_call | solution.py:167
  137.6 1.0 constant_dynamic-update-slice_fusion.2
  138.6 13.2 %collective-permute-done.3 = bf16[704,512]{1,0:T(8,128)(2,1)S(1)} collective-permute-done((bf16[704,512]{1,0:T(8,128)(2,1)S(1)}, bf16[704,512]{1,0:T(8,128)(2,1)S(1)}, u32[]{:S(2)}, u32[]{:S(2)}) %collective-permute-start.3) | collective-permute-done | bytes 720928 | tf_op jit(solution)/shard_map/ppermute | solution.py:305
  151.8 0.9 constant_dynamic-update-slice_fusion.1
  152.7 9.9 %collective-permute-done.4 = bf16[704,512]{1,0:T(8,128)(2,1)} collective-permute-done((bf16[704,512]{1,0:T(8,128)(2,1)S(1)}, bf16[704,512]{1,0:T(8,128)(2,1)}, u32[]{:S(2)}, u32[]{:S(2)}) %collective-permute-start.4) | collective-permute-done | bytes 720928 | tf_op jit(solution)/shard_map/ppermute | solution.py:305
  162.6 2.1 constant_dynamic-update-slice_fusion
  164.7 40.9 %all-gather.2.cloned.1.call-done = bf16[2048,1408]{1,0:T(8,128)(2,1)} async-done(((bf16[512,1408]{1,0:T(8,128)(2,1)}), bf16[2048,1408]{1,0:T(8,128)(2,1)}) %all-gather.2.cloned.1.call-update) | async-done | bytes 5767184 | tf_op jit(solution)/shard_map/all_gather | solution.py:295
  205.6 6.4 %fusion.55 = f32[512,1408]{1,0:T(8,128)S(1)} fusion(bf16[512,2048]{1,0:T(8,128)(2,1)} %bitcast.86, bf16[2048,1408]{1,0:T(8,128)(2,1)} %all-gather.2.cloned.1.call-done), kind=kOutput, calls=%fused_computation.105 | convolution fusion | flops 2952790016 | bytes 10747904 | tf_op jit(solution)/shard_map/dot_general | solution.py:370
  212.0 5.0 %convolution_convert_fusion = bf16[512,2048]{1,0:T(8,128)(2,1)} fusion(bf16[704,2048]{1,0:T(8,128)(2,1)} %constant_dynamic-update-slice_fusion, f32[512,1408]{1,0:T(8,128)S(1)} %fusion.55), kind=kOutput, calls=%fused_computation.23 | convolution fusion | flops 1479606272 | bytes 8126464 | tf_op jit(solution)/shard_map/dot_general | solution.py:373
  217.1 40.4 %last_stage.1 = bf16[4,64,2048]{2,1,0:T(8,128)(2,1)} custom-call(bf16[8,64,2048]{2,1,0:T(8,128)(2,1)} %bitcast.71, f32[64,2048]{1,0:T(8,128)} %get-tuple-element.156.resid_ref), custom_call_target="tpu_custom_call" | custom-call | tf_op jit(solution)/shard_map/last_stage/pallas_call | solution.py:242
  257.5 2.3 copy.59
  (53 shorter events, 0.7 us)
Async XLA Ops:
  6.5 81.5 %copy-start = (bf16[256,2048]{1,0:T(8,128)(2,1)S(1)}, bf16[256,2048]{1,0:T(8,128)(2,1)}, u32[]{:S(2)}) copy-start(bf16[256,2048]{1,0:T(8,128)(2,1)} %param.23) | copy-start | bytes 3145732
  6.5 199.1 %all-gather.2.cloned.1.call-start = ((), (), s32[]{:S(2)}) async-start(), calls=%async_computation | async-start | bytes 7208960 | tf_op jit(solution)/shard_map/all_gather | solution.py:295
  9.0 18.0 %collective-permute-start = (bf16[256,1408]{1,0:T(8,128)(2,1)S(1)}, bf16[256,1408]{1,0:T(8,128)(2,1)S(1)}, u32[]{:S(2)}, u32[]{:S(2)}) collective-permute-start(bf16[256,1408]{1,0:T(8,128)(2,1)S(1)} %pad_maximum_fusion.2), channel_id=1, source_target_pairs={{0,4},{4,0},{8,12},{12,8},{16,20},{20,16},{24,28},{28,24},{1,5},{5... | collective-permute-start | bytes 2162696 | tf_op jit(solution)/shard_map/ppermute | solution.py:264
  27.3 1.3 copy-start.1
  27.3 2.6 copy-start.3
  27.4 3.0 %copy-start.7 = (f32[64]{0:T(128)S(1)}, f32[64]{0:T(128)}, u32[]{:S(2)}) copy-start(f32[64]{0:T(128)} %param.21) | copy-start | bytes 772
  27.4 4.0 %copy-start.5 = (bf16[256,64]{0,1:T(8,128)(2,1)S(1)}, bf16[256,64]{0,1:T(8,128)(2,1)}, u32[]{:S(2)}) copy-start(bf16[256,64]{0,1:T(8,128)(2,1)} %param.18) | copy-start | bytes 98308
  27.4 4.1 %copy-start.6 = (bf16[256,64]{0,1:T(8,128)(2,1)S(1)}, bf16[256,64]{0,1:T(8,128)(2,1)}, u32[]{:S(2)}) copy-start(bf16[256,64]{0,1:T(8,128)(2,1)} %param.19) | copy-start | bytes 98308
  28.6 3.1 %copy-start.8 = (f32[64]{0:T(128)S(1)}, f32[64]{0:T(128)}, u32[]{:S(2)}) copy-start(f32[64]{0:T(128)} %param.22) | copy-start | bytes 772
  28.6 5.2 %copy-start.4 = (s32[256]{0:T(256)S(1)}, s32[256]{0:T(256)}, u32[]{:S(2)}) copy-start(s32[256]{0:T(256)} %param.20) | copy-start | bytes 3076
  28.7 28.2 %collective-permute-start.1 = (bf16[704,256]{1,0:T(8,128)(2,1)S(1)}, bf16[704,256]{1,0:T(8,128)(2,1)S(1)}, u32[]{:S(2)}, u32[]{:S(2)}) collective-permute-start(bf16[704,256]{1,0:T(8,128)(2,1)S(1)} %constant_dynamic-slice_fusion.2), channel_id=1, source_target_pairs={{0,4},{4,0},{8,12},{12,8},{16,20},{20,16},{24,28},{28,24},{1,5},{5... | collective-permute-start | bytes 1081352 | tf_op jit(solution)/shard_map/ppermute | solution.py:264
  60.1 77.5 %collective-permute-start.2 = (bf16[704,512]{1,0:T(8,128)(2,1)S(1)}, bf16[704,512]{1,0:T(8,128)(2,1)S(1)}, u32[]{:S(2)}, u32[]{:S(2)}) collective-permute-start(bf16[704,512]{1,0:T(8,128)(2,1)S(1)} %get-tuple-element.244), channel_id=1, source_target_pairs={{0,8},{4,12},{8,16},{12,20},{16,24},{20,28},{24,0},{28,4},{1,9},{5... | collective-permute-start | bytes 2162696 | tf_op jit(solution)/shard_map/ppermute | solution.py:305
  70.0 81.8 %collective-permute-start.3 = (bf16[704,512]{1,0:T(8,128)(2,1)S(1)}, bf16[704,512]{1,0:T(8,128)(2,1)S(1)}, u32[]{:S(2)}, u32[]{:S(2)}) collective-permute-start(bf16[704,512]{1,0:T(8,128)(2,1)S(1)} %get-tuple-element.244), channel_id=1, source_target_pairs={{0,16},{4,20},{8,24},{12,28},{16,0},{20,4},{24,8},{28,12},{1,17},{... | collective-permute-start | bytes 2162696 | tf_op jit(solution)/shard_map/ppermute | solution.py:305
  75.7 1.6 copy-start.2
  83.4 1.6 copy-start.2
  86.3 76.3 %collective-permute-start.4 = (bf16[704,512]{1,0:T(8,128)(2,1)S(1)}, bf16[704,512]{1,0:T(8,128)(2,1)}, u32[]{:S(2)}, u32[]{:S(2)}) collective-permute-start(bf16[704,512]{1,0:T(8,128)(2,1)S(1)} %get-tuple-element.244), channel_id=1, source_target_pairs={{0,24},{4,28},{8,0},{12,4},{16,8},{20,12},{24,16},{28,20},{1,25},{... | collective-permute-start | bytes 2162696 | tf_op jit(solution)/shard_map/ppermute | solution.py:305
Sparse Core Ops, SparseCore 0:
  28.8 176.8 all-gather.1

commit v3 on v1

--- a/solution.py
+++ b/solution.py
@@ -292,11 +292,11 @@
     q_local = normalized_rotated(queries, query_gain, local_heads, lattice_row, lattice_column)
     q_rows = q_local.transpose(1, 0, 2).reshape(local_heads * tok_rows, head_dim)
     lanes = [[2 * j + side for j in range(n // 2)] for side in range(2)]
+    down_pair = pair_share(n, [down_weight], 0, 1)
+    down_pair, gate_own, up_own = lax.optimization_barrier((down_pair, gate_weight, up_weight))
+    down_all = lax.all_gather(down_pair, "sp", axis_index_groups=lanes, axis=1, tiled=True)
     gate_up_all = lax.all_gather(
-        pair_share(n, [gate_weight, up_weight], 1, 0), "sp", axis_index_groups=lanes, axis=0, tiled=True
-    )
-    down_all = lax.all_gather(
-        pair_share(n, [down_weight], 0, 1), "sp", axis_index_groups=lanes, axis=1, tiled=True
+        pair_share(n, [gate_own, up_own], 1, 0), "sp", axis_index_groups=lanes, axis=0, tiled=True
     )
     turned = normalized_rotated(keys, key_norm_scale, 1, lattice_row, lattice_column)
     packed = jnp.concatenate([turned.reshape(tok_rows, head_dim), values], axis=1)

time: 264 us -> 270 us (1.023)
  waiting for transfers between devices: 101 us -> 109 us
    pallas_call x1, Pallas kernels: 22.7 us -> 15 us  [gather_sp(): pl.pallas_call(functools.partial(gather_kernel, n), out_shape=(jax.ShapeD...]
    all_gather x2, waiting for transfers between devices: 77.3 us -> 84.4 us  [the longest x1 51.1 us: per_device(): lax.all_gather(down_pair, 'sp', axis_index_groups=lanes, axis=1, tiled=True)]
    pallas_call x1, Pallas kernels: 43 us -> 48.6 us  [mid_stage(): pl.pallas_call(functools.partial(mid_kernel, nt), out_shape=(jax.ShapeDty...]
  transfers between devices with their start and end apart: 4 -> 4, of which waited for: 4 -> 4; matrix products, arithmetic and copies ran while one was open for 8% -> 8% of each run, Pallas kernels for 25% -> 24%
where the time goes in v3:
time: 270 us
  waiting for transfers between devices  109 us (40%)
  Pallas kernels  104 us (39%)
  matrix products  17.6 us (7%)
  between operations  13.7 us (5%)
  local copies, waits for them, and re-layouts  8.92 us (3%)
  other arithmetic  8.05 us (3%)
  loops' own time  5.03 us (2%)
  starting transfers between devices  3.41 us (1%)
    all_gather x1, waiting for transfers between devices, per_device(): lax.all_gather(down_pair, 'sp', axis_index_groups=lanes, axis=1, tiled=True)  51.1 us
    pallas_call x1, Pallas kernels, mid_stage(): pl.pallas_call(functools.partial(mid_kernel, nt), out_shape=(jax.ShapeDty...  48.6 us
    pallas_call x1, Pallas kernels, last_stage(): pl.pallas_call(functools.partial(last_kernel, nt), out_shape=jax.ShapeDty...  40.7 us
    all_gather x1, waiting for transfers between devices, per_device(): lax.all_gather(pair_share(n, [gate_own, up_own], 1, 0), 'sp', axis_index_...  33.3 us
    ppermute x2, waiting for transfers between devices, pair_share(): came = lax.ppermute(away, 'sp', [(i, i ^ 1) for i in range(n)])  23.4 us
    pallas_call x1, Pallas kernels, gather_sp(): pl.pallas_call(functools.partial(gather_kernel, n), out_shape=(jax.ShapeD...  15 us
    dot_general x1, matrix products, per_device(): both = jnp.dot(normed, gate_up_all, preferred_element_type=jnp.float32)  8.28 us
    dot_general x1, matrix products, per_device(): fed_part = jnp.dot(hidden, down_all, preferred_element_type=jnp.float32)  5.96 us
  transfers between devices with their start and end apart: 4, of which 4 were waited for; matrix products, arithmetic and copies ran while one was open for 8% of the time, Pallas kernels for 24%

profile of v3, /device:TPU:1, one launch (start us, length us, event | category | flops | bytes accessed | tf_op | source)
XLA Modules:
  0.0 269.6 jit_solution(13924371574811810188)
XLA Ops:
  6.6 1.2 constant_dynamic-slice_fusion.6
  7.7 2.1 collective-permute-start
  9.8 8.1 %collective-permute-done = bf16[704,256]{1,0:T(8,128)(2,1)S(1)} collective-permute-done((bf16[704,256]{1,0:T(8,128)(2,1)S(1)}, bf16[704,256]{1,0:T(8,128)(2,1)S(1)}, u32[]{:S(2)}, u32[]{:S(2)}) %collective-permute-start) | collective-permute-done | bytes 360480 | tf_op jit(solution)/shard_map/ppermute | solution.py:264
  18.0 1.1 broadcast_select_fusion.3
  19.1 0.9 pad_maximum_fusion.1
  20.0 0.8 constant_dynamic-slice_fusion.4
  20.8 0.2 pad_maximum_fusion.3
  21.0 1.2 collective-permute-start.1
  22.2 15.3 %collective-permute-done.1 = bf16[256,1408]{1,0:T(8,128)(2,1)S(1)} collective-permute-done((bf16[256,1408]{1,0:T(8,128)(2,1)S(1)}, bf16[256,1408]{1,0:T(8,128)(2,1)S(1)}, u32[]{:S(2)}, u32[]{:S(2)}) %collective-permute-start.1) | collective-permute-done | bytes 720928 | tf_op jit(solution)/shard_map/ppermute | solution.py:264
  37.5 0.4 broadcast_select_fusion.1
  37.9 0.0 copy-start.3
  37.9 0.0 copy-start.7
  37.9 0.0 copy-start.5
  37.9 0.0 copy-start.6
  38.0 1.3 pad_maximum_fusion
  39.2 0.0 all-gather.3.cloned.1.call-update
  39.2 0.0 all-gather.5.cloned.1.call-start
  39.3 0.7 all-gather.5.cloned.1.call-update
  40.0 0.1 copy.29
  40.2 0.2 multiply_cosine_fusion.3
  40.4 0.1 fusion.24
  40.6 0.2 copy.33
  40.8 0.1 copy.25
  40.9 0.1 copy.28
  41.0 0.1 fusion.33
  41.2 0.1 fusion.35
  41.3 1.2 fusion.46
  42.5 0.8 concatenate.37.kv_ref
  43.3 15.0 %gather_sp.1 = (bf16[8,256,128]{2,1,0:T(8,128)(2,1)}, s32[8,1,256]{2,1,0:T(1,128)}) custom-call(bf16[256,128]{1,0:T(8,128)(2,1)} %concatenate.37.kv_ref, s32[1,256]{1,0:T(1,128)S(1)} %bitcast.84), custom_call_target="tpu_custom_call" | custom-call | tf_op jit(solution)/shard_map/gather_sp/pallas_call | solution.py:93
  58.3 0.7 reduce.2
  59.0 0.6 fusion.54
  59.6 1.4 fusion.53
  61.1 9.8 %while.15 = (s32[]{:T(128)}, f32[1024]{0:T(1024)S(1)}, f32[1024]{0:T(1024)S(1)}, f32[1024,64]{0,1:T(8,128)S(1)}, s32[2,1024]{1,0:T(2,128)S(1)}, /*index=5*/s32[]...) while((s32[]{:T(128)}, f32[1024]{0:T(1024)S(1)}, ...), condition=%wide.region_7.8_spmd.clone, body=%wide.region_2.7_spmd.clone.sunk | while | flops 285345792 | bytes 14005583 | solution.py:352
  61.1 0.6 fusion.63
  64.2 3.6 %conditional.3 = ((f32[1024]{0:T(1024)S(1)}, f32[1024]{0:T(1024)S(1)}, f32[1024,64]{0,1:T(8,128)S(1)})) conditional(s32[]{:T(128)} %convert_element_type.71, (f32[1024]{0:T(1024)S(1)}, f32[1024]{0:T(1024)S(1)}, f32[1024,64]{0,1:T(8,128)S(1)}) %tuple.66, (s32[256]{0:T(256)S(1)}, s32[1,1024]{1,0:T(1,128)S(1)}, bf16[2,1024,64]{2,1,0:T(8,128)(2,1)S(1)}, ...), branch_computations={%region_3.3_spmd, %region_4.6_spmd} | conditional | flops 285345792 | bytes 13997096 | solution.py:330
  64.2 0.7 fusion.2
  65.0 1.5 fusion.4
  66.5 1.2 fusion.7
  67.8 0.6 fusion.63
  70.9 0.1 reshape.342
  71.0 1.4 convolution_convert_fusion.1
  72.4 48.6 %mid_stage.1 = (bf16[8,64,2048]{2,1,0:T(8,128)(2,1)}, f32[64,2048]{1,0:T(8,128)}) custom-call(bf16[4,64,2048]{2,1,0:T(8,128)(2,1)} %bitcast.70, bf16[4,64,2048]{2,1,0:T(8,128)(2,1)} %bitcast.72, f32[1,2048]{1,0:T(1,128)} %bitcast.85), custom_call_target="tpu_custom_call" | custom-call | tf_op jit(solution)/shard_map/mid_stage/pallas_call | solution.py:167
  121.1 33.3 %all-gather.3.cloned.1.call-done = bf16[2048,1408]{1,0:T(8,128)(2,1)} async-done(((bf16[512,1408]{1,0:T(8,128)(2,1)}), bf16[2048,1408]{1,0:T(8,128)(2,1)}) %all-gather.3.cloned.1.call-update) | async-done | bytes 5767184 | tf_op jit(solution)/shard_map/all_gather | solution.py:298
  154.4 8.3 %fusion.55 = f32[512,1408]{1,0:T(8,128)} fusion(bf16[512,2048]{1,0:T(8,128)(2,1)} %bitcast.86, bf16[2048,1408]{1,0:T(8,128)(2,1)} %all-gather.3.cloned.1.call-done), kind=kOutput, calls=%fused_computation.101 | convolution fusion | flops 2952790016 | bytes 10747904 | tf_op jit(solution)/shard_map/dot_general | solution.py:362
  162.7 51.1 %all-gather.5.cloned.1.call-done = bf16[704,2048]{1,0:T(8,128)(2,1)} async-done(((bf16[704,512]{1,0:T(8,128)(2,1)}), bf16[704,2048]{1,0:T(8,128)(2,1)}) %all-gather.5.cloned.1.call-update) | async-done | bytes 2883600 | tf_op jit(solution)/shard_map/all_gather | solution.py:297
  213.8 6.0 %convolution_convert_fusion = bf16[512,2048]{1,0:T(8,128)(2,1)} fusion(bf16[704,2048]{1,0:T(8,128)(2,1)} %all-gather.5.cloned.1.call-done, f32[512,1408]{1,0:T(8,128)} %fusion.55), kind=kOutput, calls=%fused_computation.23 | convolution fusion | flops 1479606272 | bytes 8126464 | tf_op jit(solution)/shard_map/dot_general | solution.py:365
  219.8 40.7 %last_stage.1 = bf16[4,64,2048]{2,1,0:T(8,128)(2,1)} custom-call(bf16[8,64,2048]{2,1,0:T(8,128)(2,1)} %bitcast.71, f32[64,2048]{1,0:T(8,128)} %get-tuple-element.162.resid_ref), custom_call_target="tpu_custom_call" | custom-call | tf_op jit(solution)/shard_map/last_stage/pallas_call | solution.py:242
  260.5 2.3 copy.55
  (36 shorter events, 0.3 us)
Async XLA Ops:
  6.5 64.5 %copy-start = (bf16[256,2048]{1,0:T(8,128)(2,1)S(1)}, bf16[256,2048]{1,0:T(8,128)(2,1)}, u32[]{:S(2)}) copy-start(bf16[256,2048]{1,0:T(8,128)(2,1)} %param.23) | copy-start | bytes 3145732
  6.5 13.5 %copy-start.2 = (bf16[256,1408]{1,0:T(8,128)(2,1)S(1)}, bf16[256,1408]{1,0:T(8,128)(2,1)}, u32[]{:S(2)}) copy-start(bf16[256,1408]{1,0:T(8,128)(2,1)} %param.25) | copy-start | bytes 2162692
  6.5 13.5 %copy-start.1 = (bf16[256,1408]{1,0:T(8,128)(2,1)S(1)}, bf16[256,1408]{1,0:T(8,128)(2,1)}, u32[]{:S(2)}) copy-start(bf16[256,1408]{1,0:T(8,128)(2,1)} %param.26) | copy-start | bytes 2162692
  6.5 147.8 %all-gather.3.cloned.1.call-start = ((), (), s32[]{:S(2)}) async-start(), calls=%async_computation | async-start | bytes 7208960 | tf_op jit(solution)/shard_map/all_gather | solution.py:298
  7.7 10.2 %collective-permute-start = (bf16[704,256]{1,0:T(8,128)(2,1)S(1)}, bf16[704,256]{1,0:T(8,128)(2,1)S(1)}, u32[]{:S(2)}, u32[]{:S(2)}) collective-permute-start(bf16[704,256]{1,0:T(8,128)(2,1)S(1)} %constant_dynamic-slice_fusion.6), channel_id=1, source_target_pairs={{0,4},{4,0},{8,12},{12,8},{16,20},{20,16},{24,28},{28,24},{1,5},{5... | collective-permute-start | bytes 1081352 | tf_op jit(solution)/shard_map/ppermute | solution.py:264
  21.0 16.5 %collective-permute-start.1 = (bf16[256,1408]{1,0:T(8,128)(2,1)S(1)}, bf16[256,1408]{1,0:T(8,128)(2,1)S(1)}, u32[]{:S(2)}, u32[]{:S(2)}) collective-permute-start(bf16[256,1408]{1,0:T(8,128)(2,1)S(1)} %pad_maximum_fusion.3), channel_id=1, source_target_pairs={{0,4},{4,0},{8,12},{12,8},{16,20},{20,16},{24,28},{28,24},{1,5},{5... | collective-permute-start | bytes 2162696 | tf_op jit(solution)/shard_map/ppermute | solution.py:264
  37.9 2.1 copy-start.3
  37.9 2.5 copy-start.7
  37.9 2.8 %copy-start.5 = (bf16[256,64]{0,1:T(8,128)(2,1)S(1)}, bf16[256,64]{0,1:T(8,128)(2,1)}, u32[]{:S(2)}) copy-start(bf16[256,64]{0,1:T(8,128)(2,1)} %param.18) | copy-start | bytes 98308
  37.9 2.9 %copy-start.6 = (bf16[256,64]{0,1:T(8,128)(2,1)S(1)}, bf16[256,64]{0,1:T(8,128)(2,1)}, u32[]{:S(2)}) copy-start(bf16[256,64]{0,1:T(8,128)(2,1)} %param.19) | copy-start | bytes 98308
  39.2 1.9 copy-start.8
  39.2 4.1 %copy-start.4 = (s32[256]{0:T(256)S(1)}, s32[256]{0:T(256)}, u32[]{:S(2)}) copy-start(s32[256]{0:T(256)} %param.20) | copy-start | bytes 3076
  39.2 174.6 %all-gather.5.cloned.1.call-start = ((), (), s32[]{:S(2)}) async-start(), calls=%async_computation.1 | async-start | bytes 3604480 | tf_op jit(solution)/shard_map/all_gather | solution.py:297
Sparse Core Ops, SparseCore 0:
  39.4 114.9 all-gather.2
  155.9 57.8 all-gather.4
